TPU v7x, 32 devices: a whole 2x2x4 slice. The times are simulated.
32 devices in a mesh: rep: 2 (over x), fs: 8 (over z, y), tp: 2 (over core).
Axes of the slice: x: 2, y: 2, z: 4, core: 2. Of those that a mesh axis runs over, the one named last changes fastest.
Arguments:
- tokens: bfloat16 [6144, 2048], P(('rep', 'fs')), may hold values from -6 to 6
- first_gain: float32 [2048], replicated, may hold values from 0.1 to 1.9
- mixer_gate: bfloat16 [2048, 2048], P('fs', 'tp'), may hold values from -0.125 to 0.125
- mixer_value: bfloat16 [2048, 2048], P('fs', 'tp'), may hold values from -1 to 1
- value_gain: float32 [2048], replicated, may hold values from 0.1 to 1.9
- value_shift: float32 [2048], replicated, may hold values from -3 to 3
- spatial_weight: bfloat16 [16, 128, 128], replicated, may hold values from -0.75 to 0.75
- spatial_bias: float32 [16, 128], replicated, may hold values from 0.1 to 1.9
- mixer_out: bfloat16 [2048, 2048], P('tp', 'fs'), may hold values from -0.125 to 0.125
- second_gain: float32 [2048], replicated, may hold values from 0.1 to 1.9
- up_gate: bfloat16 [2048, 4096], P('fs', 'tp'), may hold values from -0.125 to 0.125
- up_value: bfloat16 [2048, 4096], P('fs', 'tp'), may hold values from -0.125 to 0.125
- taps_gate: float32 [3, 4096], replicated, may hold values from -3.5 to 3.5
- taps_value: float32 [3, 4096], replicated, may hold values from -3.5 to 3.5
- down_proj: bfloat16 [4096, 2048], P('tp', 'fs'), may hold values from -0.09375 to 0.09375
Outputs:
- layer_out: bfloat16 [6144, 2048], P(('rep', 'fs'))
All inputs are finite; a program needn't handle non-finite values.
Results may differ from a plain program's by a relative error of at most 0.015.
Values may be sent and summed in bfloat16 or wider, within the bound.
No kernel may reach another device: no remote copies, remote signals or barrier semaphores. Data moves between devices by JAX's collectives and lax.ppermute only.
A program may use at most 64 MiB of HBM per device.

v0:
```python
import jax
import jax.numpy as jnp
from jax import lax
from jax.sharding import PartitionSpec as P

D = 2048
GDIM = 128
BLK = 128
LEN = 128


def normalize(matrix, scale_gain):
    values = matrix.astype(jnp.float32)
    factor = lax.rsqrt(jnp.mean(values * values, axis=-1, keepdims=True) + 1e-06)
    return (values * factor * scale_gain).astype(jnp.bfloat16)


def causal_conv(values, tap_weights):
    by_sequence = values.reshape(-1, LEN, values.shape[-1])
    padded = jnp.pad(by_sequence, ((0, 0), (2, 0), (0, 0)))
    summed = (
        tap_weights[0] * padded[:, 0:LEN]
        + tap_weights[1] * padded[:, 1 : LEN + 1]
        + tap_weights[2] * padded[:, 2 : LEN + 2]
    )
    return summed.reshape(values.shape)


def local(
    tokens,
    first_gain,
    mixer_gate,
    mixer_value,
    value_gain,
    value_shift,
    spatial_weight,
    spatial_bias,
    mixer_out,
    second_gain,
    up_gate,
    up_value,
    taps_gate,
    taps_value,
    down_proj,
):
    tp_index = lax.axis_index("tp")
    first = normalize(tokens, first_gain)
    row_count = first.shape[0]
    local_cols = mixer_gate.shape[1]
    gate_acc = jnp.dot(
        first,
        lax.all_gather(mixer_gate, "fs", axis=0, tiled=True),
        preferred_element_type=jnp.float32,
    )
    value_acc = jnp.dot(
        first,
        lax.all_gather(mixer_value, "fs", axis=0, tiled=True),
        preferred_element_type=jnp.float32,
    )
    gate_act = jax.nn.gelu(gate_acc)
    value_act = jax.nn.gelu(value_acc)
    value_sum, value_squares = lax.psum(
        (jnp.sum(value_act, axis=1), jnp.sum(value_act * value_act, axis=1)), "tp"
    )
    row_mean = value_sum / D
    variance = value_squares / D - row_mean * row_mean
    col_gain = lax.dynamic_slice_in_dim(value_gain, tp_index * local_cols, local_cols)
    col_shift = lax.dynamic_slice_in_dim(value_shift, tp_index * local_cols, local_cols)
    centred = (
        (value_act - row_mean[:, None]) * lax.rsqrt(variance[:, None] + 1e-05) * col_gain
        + col_shift
    ).astype(jnp.bfloat16)
    local_groups = local_cols // GDIM
    local_weights = lax.dynamic_slice_in_dim(
        spatial_weight, tp_index * local_groups, local_groups, 0
    )
    biases = lax.dynamic_slice_in_dim(spatial_bias, tp_index * local_groups, local_groups, 0)
    masked = local_weights * jnp.tril(jnp.ones((BLK, BLK), jnp.bfloat16))
    blocks = centred.reshape(row_count // BLK, BLK, local_groups, GDIM)
    mixed_rows = (
        jnp.einsum("gts,bsgc->btgc", masked, blocks, preferred_element_type=jnp.float32)
        + biases.T[None, :, :, None]
    )
    gated_rows = (gate_act * mixed_rows.reshape(row_count, local_cols)).astype(jnp.bfloat16)
    whole_out = lax.all_gather(mixer_out, "fs", axis=1, tiled=True)
    row_share = row_count // lax.axis_size("tp")
    summed = lax.psum(
        jnp.dot(gated_rows, whole_out, preferred_element_type=jnp.float32).astype(jnp.bfloat16),
        "tp",
    ).astype(jnp.float32)
    residual = (tokens.astype(jnp.float32) + summed).astype(jnp.bfloat16)
    second = normalize(residual, second_gain)
    kept_rows = lax.dynamic_slice_in_dim(residual, tp_index * row_share, row_share, 0)
    hidden_cols = up_gate.shape[1]

    def add_rows(portion):
        return jnp.dot(second, portion, preferred_element_type=jnp.float32)

    gate_up = add_rows(lax.all_gather(up_gate, "fs", axis=0, tiled=True))
    value_up = add_rows(lax.all_gather(up_value, "fs", axis=0, tiled=True))
    gate_taps = lax.dynamic_slice_in_dim(taps_gate, tp_index * hidden_cols, hidden_cols, 1)
    value_taps = lax.dynamic_slice_in_dim(taps_value, tp_index * hidden_cols, hidden_cols, 1)
    hidden = (
        jax.nn.silu(causal_conv(gate_up, gate_taps)) * causal_conv(value_up, value_taps)
    ).astype(jnp.bfloat16)
    whole_down = lax.all_gather(down_proj, "fs", axis=1, tiled=True)
    ffn_total = lax.psum_scatter(
        jnp.dot(hidden, whole_down, preferred_element_type=jnp.float32).astype(jnp.bfloat16),
        "tp",
        scatter_dimension=0,
        tiled=True,
    ).astype(jnp.float32)
    final_rows = (kept_rows.astype(jnp.float32) + ffn_total).astype(jnp.bfloat16)
    return lax.all_gather(final_rows, "tp", axis=0, tiled=True)


def solution(mesh):
    in_specs = (
        P(("rep", "fs"), None),
        P(),
        P("fs", "tp"),
        P("fs", "tp"),
        P(),
        P(),
        P(),
        P(),
        P("tp", "fs"),
        P(),
        P("fs", "tp"),
        P("fs", "tp"),
        P(),
        P(),
        P("tp", "fs"),
    )
    out_specs = P(("rep", "fs"), None)
    return jax.shard_map(local, mesh=mesh, in_specs=in_specs, out_specs=out_specs, check_vma=False)
```

profile of v0, /device:TPU:0, one launch (start us, length us, event | category | flops | bytes accessed | tf_op | source)
XLA Modules:
  0.0 677.7 jit_solution(8803535783752608188)
XLA Ops:
  6.5 0.0 copy-start
  6.5 0.0 copy-start.2
  6.5 0.0 copy-start.6
  6.5 0.0 all-gather.10.cloned.1.call-start
  6.5 0.7 all-gather.10.cloned.1.call-update
  7.3 0.0 all-gather.12.cloned.1.call-start
  7.3 0.7 all-gather.12.cloned.1.call-update
  8.0 0.0 all-gather.8.cloned.1.call-start
  8.1 0.7 all-gather.8.cloned.1.call-update
  8.7 0.0 all-reduce.5.cloned.1.call-start
  8.8 0.0 copy-done
  8.8 1.8 fusion.11
  10.6 0.0 dynamic-slice-start
  10.7 0.0 dynamic-slice-start.1
  10.7 74.3 %all-gather.10.cloned.1.call-done = bf16[2048,1024]{1,0:T(8,128)(2,1)} async-done(((bf16[256,1024]{1,0:T(8,128)(2,1)}), bf16[2048,1024]{1,0:T(8,128)(2,1)}) %all-gather.10.cloned.1.call-update) | async-done | bytes 4194320 | tf_op jit(solution)/shard_map/all_gather | solution.py:57
  85.0 0.0 copy-done.2
  85.0 0.0 copy-done.6
  85.0 4.5 fusion.66
  89.6 2.5 all-reduce.2
  92.0 0.0 copy-start.5
  92.0 0.0 dynamic-slice-done
  92.0 0.0 dynamic-slice-done.1
  92.1 0.4 fusion.35
  92.4 0.2 copy.19
  92.6 0.5 copy-done.5
  93.1 0.4 bitcast_add_fusion
  93.5 1.6 copy.17
  95.2 65.1 %all-gather.12.cloned.1.call-done = bf16[1024,2048]{1,0:T(8,128)(2,1)} async-done(((bf16[1024,256]{1,0:T(8,128)(2,1)}), bf16[1024,2048]{1,0:T(8,128)(2,1)}) %all-gather.12.cloned.1.call-update) | async-done | bytes 4194320 | tf_op jit(solution)/shard_map/all_gather | solution.py:85
  160.3 73.1 %all-gather.8.cloned.1.call-done = bf16[2048,1024]{1,0:T(8,128)(2,1)} async-done(((bf16[256,1024]{1,0:T(8,128)(2,1)}), bf16[2048,1024]{1,0:T(8,128)(2,1)}) %all-gather.8.cloned.1.call-update) | async-done | bytes 4194320 | tf_op jit(solution)/shard_map/all_gather | solution.py:52
  233.4 9.0 %convolution_convert_fusion.1 = bf16[384,2048]{1,0:T(8,128)(2,1)} fusion(bf16[1024,2048]{1,0:T(8,128)(2,1)} %all-gather.12.cloned.1.call-done, f32[48,8,8,128]{3,2,1,0:T(8,128)} %bitcast.53, bf16[2048,1024]{1,0:T(8,128)(2,1)} %all-gather.8.cloned.1.call-done, bf16[384,2048]{1,0:T(8,128)(2,1)S(1)} %copy-done.2, f32[2048]{0:T(1024)S(1)} %copy-done.6, ...), kind=kOutput, calls=%fused_computation.32 | convolution fusion | flops 3229089792 | bytes 13116928 | tf_op jit(solution)/shard_map/dot_general | solution.py:88
  242.4 0.0 all-reduce.5.cloned.1.call-update
  242.5 0.0 all-gather.14.cloned.1.call-start
  242.5 0.5 all-gather.14.cloned.1.call-update
  243.0 0.0 all-gather.16.cloned.1.call-start
  243.1 0.5 all-gather.16.cloned.1.call-update
  243.6 0.0 copy-start.7
  243.6 0.0 all-gather.18.cloned.1.call-start
  243.7 0.7 all-gather.18.cloned.1.call-update
  244.4 0.2 reduce-scatter.2.cloned.1.call-start
  244.6 1.0 constant_dynamic-slice_fusion
  245.6 15.9 %all-reduce.5.cloned.1.call-done = bf16[384,2048]{1,0:T(8,128)(2,1)} async-done(((bf16[384,2048]{1,0:T(8,128)(2,1)}), bf16[384,2048]{1,0:T(8,128)(2,1)}) %all-reduce.5.cloned.1.call-update) | async-done | bytes 1572880 | tf_op jit(solution)/shard_map/psum | solution.py:87
  261.5 2.2 fusion.8
  263.7 0.0 copy-start.3
  263.7 125.5 %all-gather.14.cloned.1.call-done = bf16[2048,2048]{1,0:T(8,128)(2,1)} async-done(((bf16[256,2048]{1,0:T(8,128)(2,1)}), bf16[2048,2048]{1,0:T(8,128)(2,1)}) %all-gather.14.cloned.1.call-update) | async-done | bytes 8388624 | tf_op jit(solution)/shard_map/all_gather | solution.py:99
  389.2 0.0 copy-done.7
  389.2 5.9 fusion.54
  395.1 0.0 copy-done.3
  395.1 0.9 fusion.2
  396.1 117.8 %all-gather.16.cloned.1.call-done = bf16[2048,2048]{1,0:T(8,128)(2,1)} async-done(((bf16[256,2048]{1,0:T(8,128)(2,1)}), bf16[2048,2048]{1,0:T(8,128)(2,1)}) %all-gather.16.cloned.1.call-update) | async-done | bytes 8388624 | tf_op jit(solution)/shard_map/all_gather | solution.py:100
  513.8 6.4 fusion.52
  520.2 0.9 fusion.6
  521.2 2.2 fusion.15
  523.3 115.7 %all-gather.18.cloned.1.call-done = bf16[2048,2048]{1,0:T(8,128)(2,1)} async-done(((bf16[2048,256]{1,0:T(8,128)(2,1)}), bf16[2048,2048]{1,0:T(8,128)(2,1)}) %all-gather.18.cloned.1.call-update) | async-done | bytes 8388624 | tf_op jit(solution)/shard_map/all_gather | solution.py:106
  639.0 8.5 %convolution_convert_fusion = bf16[384,2048]{1,0:T(8,128)(2,1)} fusion(bf16[384,2048]{1,0:T(8,128)(2,1)} %fusion.15, bf16[2048,2048]{1,0:T(8,128)(2,1)} %all-gather.18.cloned.1.call-done), kind=kOutput, calls=%fused_computation.31 | convolution fusion | flops 3222011904 | bytes 11534336 | tf_op jit(solution)/shard_map/dot_general | solution.py:108
  647.5 0.0 reduce-scatter.2.cloned.1.call-update
  647.5 0.0 all-gather.20.cloned.1.call-start
  647.6 0.0 copy-start.1
  647.6 7.3 %reduce-scatter.2.cloned.1.call-done = bf16[192,2048]{1,0:T(8,128)(2,1)} async-done(((bf16[384,2048]{1,0:T(8,128)(2,1)}), bf16[192,2048]{1,0:T(8,128)(2,1)}) %reduce-scatter.2.cloned.1.call-update) | async-done | bytes 786448 | tf_op jit(solution)/shard_map/reduce_scatter | solution.py:107
  654.9 0.0 copy-done.4
  654.9 2.3 add_convert_fusion
  657.2 0.0 all-gather.20.cloned.1.call-update
  657.2 11.2 %all-gather.20.cloned.1.call-done = bf16[384,2048]{1,0:T(8,128)(2,1)} async-done(((bf16[192,2048]{1,0:T(8,128)(2,1)}), bf16[384,2048]{1,0:T(8,128)(2,1)}) %all-gather.20.cloned.1.call-update) | async-done | bytes 1572880 | tf_op jit(solution)/shard_map/all_gather | solution.py:114
  668.5 2.7 copy.27
  671.2 0.0 copy-done.1
  (6 shorter events, 0.0 us)
Async XLA Ops:
  6.5 2.3 copy-start
  6.5 78.5 %copy-start.2 = (bf16[384,2048]{1,0:T(8,128)(2,1)S(1)}, bf16[384,2048]{1,0:T(8,128)(2,1)}, u32[]{:S(2)}) copy-start(bf16[384,2048]{1,0:T(8,128)(2,1)} %param.15) | copy-start | bytes 4718596
  6.5 78.5 %copy-start.6 = (f32[2048]{0:T(1024)S(1)}, f32[2048]{0:T(1024)}, u32[]{:S(2)}) copy-start(f32[2048]{0:T(1024)} %param.16) | copy-start | bytes 24580
  6.5 78.5 %all-gather.10.cloned.1.call-start = ((), (), s32[]{:S(2)}) async-start(), calls=%async_computation.2 | async-start | bytes 4718592 | tf_op jit(solution)/shard_map/all_gather | solution.py:57
  7.3 153.0 %all-gather.12.cloned.1.call-start = ((), (), s32[]{:S(2)}) async-start(), calls=%async_computation.3 | async-start | bytes 4718592 | tf_op jit(solution)/shard_map/all_gather | solution.py:85
  8.0 225.4 %all-gather.8.cloned.1.call-start = ((), (), s32[]{:S(2)}) async-start(), calls=%async_computation.1 | async-start | bytes 4718592 | tf_op jit(solution)/shard_map/all_gather | solution.py:52
  8.7 252.8 %all-reduce.5.cloned.1.call-start = ((), (), s32[]{:S(2)}) async-start(), calls=%async_computation.4 | async-start | bytes 3145728 | tf_op jit(solution)/shard_map/psum | solution.py:87
  10.6 81.4 %dynamic-slice-start = ((f32[2048]{0:T(1024)}, s32[]{:T(128)}), f32[1024]{0:T(1024)S(1)}, s32[]{:S(2)}) async-start(f32[2048]{0:T(1024)} %param.19, s32[]{:T(128)} %select_n.23), calls=%async_computation.10 | async-start | bytes 8704 | tf_op jit(solution)/shard_map/dynamic_slice | solution.py:67
  10.7 81.4 %dynamic-slice-start.1 = ((f32[2048]{0:T(1024)}, s32[]{:T(128)}), f32[1024]{0:T(1024)S(1)}, s32[]{:S(2)}) async-start(f32[2048]{0:T(1024)} %param.20, s32[]{:T(128)} %select_n.23), calls=%async_computation.11 | async-start | bytes 8704 | tf_op jit(solution)/shard_map/dynamic_slice | solution.py:68
  92.0 1.1 copy-start.5
  242.5 146.7 %all-gather.14.cloned.1.call-start = ((), (), s32[]{:S(2)}) async-start(), calls=%async_computation.5 | async-start | bytes 9437184 | tf_op jit(solution)/shard_map/all_gather | solution.py:99
  243.0 270.8 %all-gather.16.cloned.1.call-start = ((), (), s32[]{:S(2)}) async-start(), calls=%async_computation.6 | async-start | bytes 9437184 | tf_op jit(solution)/shard_map/all_gather | solution.py:100
  243.6 145.6 %copy-start.7 = (f32[2048]{0:T(1024)S(1)}, f32[2048]{0:T(1024)}, u32[]{:S(2)}) copy-start(f32[2048]{0:T(1024)} %param.24) | copy-start | bytes 24580
  243.6 395.4 %all-gather.18.cloned.1.call-start = ((), (), s32[]{:S(2)}) async-start(), calls=%async_computation.7 | async-start | bytes 9437184 | tf_op jit(solution)/shard_map/all_gather | solution.py:106
  244.4 410.5 %reduce-scatter.2.cloned.1.call-start = ((), (), s32[]{:S(2)}) async-start(), calls=%async_computation.8 | async-start | bytes 2359296 | tf_op jit(solution)/shard_map/reduce_scatter | solution.py:107
  263.7 131.5 %copy-start.3 = (bf16[384,2048]{1,0:T(8,128)(2,1)}, bf16[384,2048]{1,0:T(8,128)(2,1)S(1)}, u32[]{:S(2)}) copy-start(bf16[384,2048]{1,0:T(8,128)(2,1)S(1)} %get-tuple-element.10) | copy-start | bytes 4718596
  523.3 131.6 %copy-start.4 = (bf16[384,2048]{1,0:T(8,128)(2,1)S(1)}, bf16[384,2048]{1,0:T(8,128)(2,1)}, u32[]{:S(2)}) copy-start(bf16[384,2048]{1,0:T(8,128)(2,1)} %copy-done.3) | copy-start | bytes 4718596
  647.5 20.9 %all-gather.20.cloned.1.call-start = ((), (), s32[]{:S(2)}) async-start(), calls=%async_computation.9 | async-start | bytes 2359296 | tf_op jit(solution)/shard_map/all_gather | solution.py:114
  647.6 23.6 %copy-start.1 = (f32[16,128]{1,0:T(8,128)S(1)}, f32[16,128]{1,0:T(8,128)}, u32[]{:S(2)}) copy-start(f32[16,128]{1,0:T(8,128)} %param.22) | copy-start | bytes 24580
Sparse Core Ops, SparseCore 0:
  9.5 75.5 all-gather.9
  87.1 73.1 all-gather.11
  162.4 70.9 all-gather.7
  242.6 18.8 all-reduce.4
  263.5 125.6 all-gather.13
  391.2 122.6 all-gather.15
  515.9 123.1 all-gather.17
  647.7 7.2 reduce-scatter.1
  657.3 11.0 all-gather.19
where the time goes:
time: 678 us
  waiting for transfers between devices  610 us (90%)
  matrix products  34.8 us (5%)
  between operations  13.4 us (2%)
  other arithmetic  10.6 us (2%)
    all_gather x1, waiting for transfers between devices, local(): gate_up = add_rows(lax.all_gather(up_gate, 'fs', axis=0, tiled=True))  125 us
    all_gather x1, waiting for transfers between devices, local(): value_up = add_rows(lax.all_gather(up_value, 'fs', axis=0, tiled=True))  118 us
    all_gather x1, waiting for transfers between devices, local(): whole_down = lax.all_gather(down_proj, 'fs', axis=1, tiled=True)  116 us
    all_gather x1, waiting for transfers between devices, local(): lax.all_gather(mixer_value, 'fs', axis=0, tiled=True)  74.3 us
    all_gather x1, waiting for transfers between devices, local(): lax.all_gather(mixer_gate, 'fs', axis=0, tiled=True)  73.1 us
    all_gather x1, waiting for transfers between devices, local(): whole_out = lax.all_gather(mixer_out, 'fs', axis=1, tiled=True)  65.1 us
    psum x1, waiting for transfers between devices, local(): lax.psum(jnp.dot(gated_rows, whole_out, preferred_element_type=jnp.float3...  15.9 us
  transfers between devices with their start and end apart: 9, of which 9 were waited for; matrix products, arithmetic and copies ran while one was open for 4% of the time, Pallas kernels for 0%

commit v1 on v0

--- a/solution.py
+++ b/solution.py
@@ -82,7 +82,13 @@
         + biases.T[None, :, :, None]
     )
     gated_rows = (gate_act * mixed_rows.reshape(row_count, local_cols)).astype(jnp.bfloat16)
-    whole_out = lax.all_gather(mixer_out, "fs", axis=1, tiled=True)
+    peers = lax.axis_size("fs")
+    held, tiles = (mixer_out, [mixer_out])
+    for _ in range(peers - 1):
+        held = lax.ppermute(held, "fs", [(i, (i + 1) % peers) for i in range(peers)])
+        tiles.insert(0, held)
+    line = jnp.concatenate(tiles, axis=1)
+    whole_out = jnp.roll(line, (lax.axis_index("fs") + 1) * mixer_out.shape[1], axis=1)
     row_share = row_count // lax.axis_size("tp")
     summed = lax.psum(
         jnp.dot(gated_rows, whole_out, preferred_element_type=jnp.float32).astype(jnp.bfloat16),

time: 678 us -> 652 us (0.962)
  waiting for transfers between devices: 610 us -> 565 us
  local copies, waits for them, and re-layouts: 6.08 us -> 20.2 us
    ppermute x0 -> x7, waiting for transfers between devices: none -> 153 us  [local(): lax.ppermute(held, 'fs', [(i, (i + 1) % peers) for i in range(peers)])]
    all_gather x1, waiting for transfers between devices: 74.3 us -> 0.01 us  [local(): lax.all_gather(mixer_value, 'fs', axis=0, tiled=True)]
    all_gather x1 -> x0, waiting for transfers between devices: 65.1 us -> none  [local(): whole_out = lax.all_gather(mixer_out, 'fs', axis=1, tiled=True)]
    all_gather x1, waiting for transfers between devices: 73.1 us -> 15.2 us  [local(): lax.all_gather(mixer_gate, 'fs', axis=0, tiled=True)]
    unnamed x18 -> x43, local copies, waits for them, and re-layouts: 3.44 us -> 16.7 us
  transfers between devices with their start and end apart: 9 -> 15, of which waited for: 9 -> 14; matrix products, arithmetic and copies ran while one was open for 4% -> 7% of each run, Pallas kernels for 0% -> 0%
where the time goes in v1:
time: 652 us; the launch traced here: 651 us
  waiting for transfers between devices  565 us (87%)
  matrix products  34.8 us (5%)
  local copies, waits for them, and re-layouts  20.2 us (3%)
  between operations  13.7 us (2%)
  other arithmetic  10.7 us (2%)
    ppermute x7, waiting for transfers between devices, local(): lax.ppermute(held, 'fs', [(i, (i + 1) % peers) for i in range(peers)])  153 us
    all_gather x1, waiting for transfers between devices, local(): gate_up = add_rows(lax.all_gather(up_gate, 'fs', axis=0, tiled=True))  125 us
    all_gather x1, waiting for transfers between devices, local(): value_up = add_rows(lax.all_gather(up_value, 'fs', axis=0, tiled=True))  118 us
    all_gather x1, waiting for transfers between devices, local(): whole_down = lax.all_gather(down_proj, 'fs', axis=1, tiled=True)  116 us
    unnamed x43, local copies, waits for them, and re-layouts  16.7 us
    psum x1, waiting for transfers between devices, local(): lax.psum(jnp.dot(gated_rows, whole_out, preferred_element_type=jnp.float3...  16.1 us
    all_gather x1, waiting for transfers between devices, local(): lax.all_gather(mixer_gate, 'fs', axis=0, tiled=True)  15.2 us
  transfers between devices with their start and end apart: 15, of which 14 were waited for; matrix products, arithmetic and copies ran while one was open for 7% of the time, Pallas kernels for 0%

profile of v1, /device:TPU:0, one launch (start us, length us, event | category | flops | bytes accessed | tf_op | source)
XLA Modules:
  0.0 651.3 jit_solution(12675379626138669287)
XLA Ops:
  6.5 0.7 all-gather.9.cloned.1.call-update
  7.3 0.0 all-gather.7.cloned.1.call-start
  7.3 0.7 all-gather.7.cloned.1.call-update
  8.0 0.0 all-reduce.5.cloned.1.call-start
  8.1 3.0 collective-permute-start
  11.1 15.7 %collective-permute-done = bf16[1024,256]{1,0:T(8,128)(2,1)S(1)} collective-permute-done((bf16[1024,256]{1,0:T(8,128)(2,1)}, bf16[1024,256]{1,0:T(8,128)(2,1)S(1)}, u32[]{:S(2)}, u32[]{:S(2)}) %collective-permute-start) | collective-permute-done | bytes 524320 | tf_op jit(solution)/shard_map/ppermute | solution.py:88
  26.8 1.0 collective-permute-start.1
  27.8 26.6 %collective-permute-done.1 = bf16[1024,256]{1,0:T(8,128)(2,1)S(1)} collective-permute-done((bf16[1024,256]{1,0:T(8,128)(2,1)S(1)}, bf16[1024,256]{1,0:T(8,128)(2,1)S(1)}, u32[]{:S(2)}, u32[]{:S(2)}) %collective-permute-start.1) | collective-permute-done | bytes 524320 | tf_op jit(solution)/shard_map/ppermute | solution.py:88
  54.4 25.6 %collective-permute-done.2 = bf16[1024,256]{1,0:T(8,128)(2,1)S(1)} collective-permute-done((bf16[1024,256]{1,0:T(8,128)(2,1)S(1)}, bf16[1024,256]{1,0:T(8,128)(2,1)S(1)}, u32[]{:S(2)}, u32[]{:S(2)}) %collective-permute-start.2) | collective-permute-done | bytes 524320 | tf_op jit(solution)/shard_map/ppermute | solution.py:88
  80.0 26.9 %collective-permute-done.3 = bf16[1024,256]{1,0:T(8,128)(2,1)S(1)} collective-permute-done((bf16[1024,256]{1,0:T(8,128)(2,1)S(1)}, bf16[1024,256]{1,0:T(8,128)(2,1)S(1)}, u32[]{:S(2)}, u32[]{:S(2)}) %collective-permute-start.3) | collective-permute-done | bytes 524320 | tf_op jit(solution)/shard_map/ppermute | solution.py:88
  106.9 18.7 %collective-permute-done.4 = bf16[1024,256]{1,0:T(8,128)(2,1)S(1)} collective-permute-done((bf16[1024,256]{1,0:T(8,128)(2,1)S(1)}, bf16[1024,256]{1,0:T(8,128)(2,1)S(1)}, u32[]{:S(2)}, u32[]{:S(2)}) %collective-permute-start.4) | collective-permute-done | bytes 524320 | tf_op jit(solution)/shard_map/ppermute | solution.py:88
  125.6 22.1 %collective-permute-done.5 = bf16[1024,256]{1,0:T(8,128)(2,1)S(1)} collective-permute-done((bf16[1024,256]{1,0:T(8,128)(2,1)S(1)}, bf16[1024,256]{1,0:T(8,128)(2,1)S(1)}, u32[]{:S(2)}, u32[]{:S(2)}) %collective-permute-start.5) | collective-permute-done | bytes 524320 | tf_op jit(solution)/shard_map/ppermute | solution.py:88
  147.7 1.8 fusion.13
  149.5 17.8 %collective-permute-done.6 = bf16[1024,256]{1,0:T(8,128)(2,1)S(1)} collective-permute-done((bf16[1024,256]{1,0:T(8,128)(2,1)S(1)}, bf16[1024,256]{1,0:T(8,128)(2,1)S(1)}, u32[]{:S(2)}, u32[]{:S(2)}) %collective-permute-start.6) | collective-permute-done | bytes 524320 | tf_op jit(solution)/shard_map/ppermute | solution.py:88
  167.3 0.9 constant_dynamic-update-slice_fusion.15
  168.2 0.9 constant_dynamic-update-slice_fusion.14
  169.0 0.9 constant_dynamic-update-slice_fusion.13
  169.9 0.9 constant_dynamic-update-slice_fusion.12
  170.8 0.9 constant_dynamic-update-slice_fusion.11
  171.7 0.9 constant_dynamic-update-slice_fusion.10
  172.6 0.9 constant_dynamic-update-slice_fusion.9
  173.5 0.9 constant_dynamic-update-slice_fusion.8
  174.3 0.9 constant_dynamic-update-slice_fusion.7
  175.2 0.9 constant_dynamic-update-slice_fusion.6
  176.1 0.9 constant_dynamic-update-slice_fusion.5
  177.1 0.9 constant_dynamic-update-slice_fusion.4
  177.9 0.9 constant_dynamic-update-slice_fusion.3
  178.8 0.9 constant_dynamic-update-slice_fusion.2
  179.7 0.9 constant_dynamic-update-slice_fusion.1
  180.6 0.9 constant_dynamic-update-slice_fusion
  181.5 4.6 fusion.72
  186.1 2.5 all-reduce.2
  188.6 0.4 fusion.40
  189.0 0.2 copy.19
  189.1 0.5 copy-done.10
  189.6 0.4 bitcast_add_fusion
  190.0 1.6 copy.17
  191.7 15.2 %all-gather.7.cloned.1.call-done = bf16[2048,1024]{1,0:T(8,128)(2,1)} async-done(((bf16[256,1024]{1,0:T(8,128)(2,1)}), bf16[2048,1024]{1,0:T(8,128)(2,1)}) %all-gather.7.cloned.1.call-update) | async-done | bytes 4194320 | tf_op jit(solution)/shard_map/all_gather | solution.py:52
  206.9 9.0 %fusion.21 = bf16[384,2048]{1,0:T(8,128)(2,1)} fusion(bf16[1024,4096]{1,0:T(8,128)(2,1)} %constant_dynamic-update-slice_fusion, s32[]{:T(128)S(6)} %select_n.40, f32[48,8,8,128]{3,2,1,0:T(8,128)} %bitcast.52, bf16[2048,1024]{1,0:T(8,128)(2,1)} %all-gather.7.cloned.1.call-done, bf16[384,2048]{1,0:T(8,128)(2,1)S(1)} %copy-done.2, f32[2048]{0:T(1024)S(1)} %copy-done.11, ...), kind=kOutput, calls=%fused_computation.34 | convolution fusion | flops 3229089792 | bytes 13116932 | tf_op jit(solution)/shard_map/dot_general | solution.py:94
  215.9 0.0 all-reduce.5.cloned.1.call-update
  215.9 0.0 all-gather.11.cloned.1.call-start
  215.9 0.5 all-gather.11.cloned.1.call-update
  216.5 0.0 all-gather.13.cloned.1.call-start
  216.5 0.5 all-gather.13.cloned.1.call-update
  217.1 0.0 all-gather.15.cloned.1.call-start
  217.1 0.5 all-gather.15.cloned.1.call-update
  217.6 0.2 reduce-scatter.2.cloned.1.call-start
  217.9 1.0 constant_dynamic-slice_fusion
  218.9 16.1 %all-reduce.5.cloned.1.call-done = bf16[384,2048]{1,0:T(8,128)(2,1)} async-done(((bf16[384,2048]{1,0:T(8,128)(2,1)}), bf16[384,2048]{1,0:T(8,128)(2,1)}) %all-reduce.5.cloned.1.call-update) | async-done | bytes 1572880 | tf_op jit(solution)/shard_map/psum | solution.py:93
  235.0 2.2 fusion.10
  237.2 125.5 %all-gather.11.cloned.1.call-done = bf16[2048,2048]{1,0:T(8,128)(2,1)} async-done(((bf16[256,2048]{1,0:T(8,128)(2,1)}), bf16[2048,2048]{1,0:T(8,128)(2,1)}) %all-gather.11.cloned.1.call-update) | async-done | bytes 8388624 | tf_op jit(solution)/shard_map/all_gather | solution.py:105
  362.6 6.0 fusion.55
  368.6 0.9 fusion.4
  369.5 117.8 %all-gather.13.cloned.1.call-done = bf16[2048,2048]{1,0:T(8,128)(2,1)} async-done(((bf16[256,2048]{1,0:T(8,128)(2,1)}), bf16[2048,2048]{1,0:T(8,128)(2,1)}) %all-gather.13.cloned.1.call-update) | async-done | bytes 8388624 | tf_op jit(solution)/shard_map/all_gather | solution.py:106
  487.3 6.4 fusion.53
  493.7 0.9 fusion.8
  494.6 2.2 fusion.17
  496.8 115.6 %all-gather.15.cloned.1.call-done = bf16[2048,2048]{1,0:T(8,128)(2,1)} async-done(((bf16[2048,256]{1,0:T(8,128)(2,1)}), bf16[2048,2048]{1,0:T(8,128)(2,1)}) %all-gather.15.cloned.1.call-update) | async-done | bytes 8388624 | tf_op jit(solution)/shard_map/all_gather | solution.py:112
  612.4 8.5 %convolution_convert_fusion = bf16[384,2048]{1,0:T(8,128)(2,1)} fusion(bf16[384,2048]{1,0:T(8,128)(2,1)} %fusion.17, bf16[2048,2048]{1,0:T(8,128)(2,1)} %all-gather.15.cloned.1.call-done), kind=kOutput, calls=%fused_computation.33 | convolution fusion | flops 3222011904 | bytes 11534336 | tf_op jit(solution)/shard_map/dot_general | solution.py:114
  620.8 0.0 all-gather.17.cloned.1.call-start
  620.9 7.3 %reduce-scatter.2.cloned.1.call-done = bf16[192,2048]{1,0:T(8,128)(2,1)} async-done(((bf16[384,2048]{1,0:T(8,128)(2,1)}), bf16[192,2048]{1,0:T(8,128)(2,1)}) %reduce-scatter.2.cloned.1.call-update) | async-done | bytes 786448 | tf_op jit(solution)/shard_map/reduce_scatter | solution.py:113
  628.2 2.3 add_convert_fusion
  630.5 11.2 %all-gather.17.cloned.1.call-done = bf16[384,2048]{1,0:T(8,128)(2,1)} async-done(((bf16[192,2048]{1,0:T(8,128)(2,1)}), bf16[384,2048]{1,0:T(8,128)(2,1)}) %all-gather.17.cloned.1.call-update) | async-done | bytes 1572880 | tf_op jit(solution)/shard_map/all_gather | solution.py:120
  641.8 2.7 copy.42
  (43 shorter events, 0.1 us)
Async XLA Ops:
  6.5 141.2 %copy-start = (f32[16,128]{1,0:T(8,128)S(1)}, f32[16,128]{1,0:T(8,128)}, u32[]{:S(2)}) copy-start(f32[16,128]{1,0:T(8,128)} %param.22) | copy-start | bytes 24580
  6.5 175.0 %all-gather.9.cloned.1.call-start = ((), (), s32[]{:S(2)}) async-start(), calls=%async_computation.2 | async-start | bytes 4718592 | tf_op jit(solution)/shard_map/all_gather | solution.py:57
  7.3 199.6 %all-gather.7.cloned.1.call-start = ((), (), s32[]{:S(2)}) async-start(), calls=%async_computation.1 | async-start | bytes 4718592 | tf_op jit(solution)/shard_map/all_gather | solution.py:52
  8.0 227.0 %all-reduce.5.cloned.1.call-start = ((), (), s32[]{:S(2)}) async-start(), calls=%async_computation.3 | async-start | bytes 3145728 | tf_op jit(solution)/shard_map/psum | solution.py:93
  8.1 18.8 %collective-permute-start = (bf16[1024,256]{1,0:T(8,128)(2,1)}, bf16[1024,256]{1,0:T(8,128)(2,1)S(1)}, u32[]{:S(2)}, u32[]{:S(2)}) collective-permute-start(bf16[1024,256]{1,0:T(8,128)(2,1)} %param.23), channel_id=1, source_target_pairs={{0,2},{2,4},{4,6},{6,8},{8,10},{10,12},{12,14},{14,0},{1,3},{3,5},... | collective-permute-start | bytes 1572872 | tf_op jit(solution)/shard_map/ppermute | solution.py:88
  26.8 27.6 %collective-permute-start.1 = (bf16[1024,256]{1,0:T(8,128)(2,1)S(1)}, bf16[1024,256]{1,0:T(8,128)(2,1)S(1)}, u32[]{:S(2)}, u32[]{:S(2)}) collective-permute-start(bf16[1024,256]{1,0:T(8,128)(2,1)S(1)} %collective-permute-done), channel_id=1, source_target_pairs={{0,2},{2,4},{4,6},{6,8},{8,10},{10,12},{12,14},{14,0},{1,3},{3,5},... | collective-permute-start | bytes 1572872 | tf_op jit(solution)/shard_map/ppermute | solution.py:88
  54.4 25.6 %collective-permute-start.2 = (bf16[1024,256]{1,0:T(8,128)(2,1)S(1)}, bf16[1024,256]{1,0:T(8,128)(2,1)S(1)}, u32[]{:S(2)}, u32[]{:S(2)}) collective-permute-start(bf16[1024,256]{1,0:T(8,128)(2,1)S(1)} %collective-permute-done.1), channel_id=1, source_target_pairs={{0,2},{2,4},{4,6},{6,8},{8,10},{10,12},{12,14},{14,0},{1,3},{3,5},... | collective-permute-start | bytes 1572872 | tf_op jit(solution)/shard_map/ppermute | solution.py:88
  80.0 26.9 %collective-permute-start.3 = (bf16[1024,256]{1,0:T(8,128)(2,1)S(1)}, bf16[1024,256]{1,0:T(8,128)(2,1)S(1)}, u32[]{:S(2)}, u32[]{:S(2)}) collective-permute-start(bf16[1024,256]{1,0:T(8,128)(2,1)S(1)} %collective-permute-done.2), channel_id=1, source_target_pairs={{0,2},{2,4},{4,6},{6,8},{8,10},{10,12},{12,14},{14,0},{1,3},{3,5},... | collective-permute-start | bytes 1572872 | tf_op jit(solution)/shard_map/ppermute | solution.py:88
  106.9 64.8 %copy-start.6 = (bf16[1024,256]{1,0:T(8,128)(2,1)}, bf16[1024,256]{1,0:T(8,128)(2,1)S(1)}, u32[]{:S(2)}) copy-start(bf16[1024,256]{1,0:T(8,128)(2,1)S(1)} %collective-permute-done.3) | copy-start | bytes 1572868
  106.9 18.7 %collective-permute-start.4 = (bf16[1024,256]{1,0:T(8,128)(2,1)S(1)}, bf16[1024,256]{1,0:T(8,128)(2,1)S(1)}, u32[]{:S(2)}, u32[]{:S(2)}) collective-permute-start(bf16[1024,256]{1,0:T(8,128)(2,1)S(1)} %collective-permute-done.3), channel_id=1, source_target_pairs={{0,2},{2,4},{4,6},{6,8},{8,10},{10,12},{12,14},{14,0},{1,3},{3,5},... | collective-permute-start | bytes 1572872 | tf_op jit(solution)/shard_map/ppermute | solution.py:88
  125.6 46.1 %copy-start.8 = (bf16[1024,256]{1,0:T(8,128)(2,1)}, bf16[1024,256]{1,0:T(8,128)(2,1)S(1)}, u32[]{:S(2)}) copy-start(bf16[1024,256]{1,0:T(8,128)(2,1)S(1)} %collective-permute-done.4) | copy-start | bytes 1572868
  125.6 22.1 %collective-permute-start.5 = (bf16[1024,256]{1,0:T(8,128)(2,1)S(1)}, bf16[1024,256]{1,0:T(8,128)(2,1)S(1)}, u32[]{:S(2)}, u32[]{:S(2)}) collective-permute-start(bf16[1024,256]{1,0:T(8,128)(2,1)S(1)} %collective-permute-done.4), channel_id=1, source_target_pairs={{0,2},{2,4},{4,6},{6,8},{8,10},{10,12},{12,14},{14,0},{1,3},{3,5},... | collective-permute-start | bytes 1572872 | tf_op jit(solution)/shard_map/ppermute | solution.py:88
  147.7 19.6 %collective-permute-start.6 = (bf16[1024,256]{1,0:T(8,128)(2,1)S(1)}, bf16[1024,256]{1,0:T(8,128)(2,1)S(1)}, u32[]{:S(2)}, u32[]{:S(2)}) collective-permute-start(bf16[1024,256]{1,0:T(8,128)(2,1)S(1)} %collective-permute-done.5), channel_id=1, source_target_pairs={{0,2},{2,4},{4,6},{6,8},{8,10},{10,12},{12,14},{14,0},{1,3},{3,5},... | collective-permute-start | bytes 1572872 | tf_op jit(solution)/shard_map/ppermute | solution.py:88
  168.2 5.3 copy-start.5
  172.6 3.5 copy-start.9
  172.6 4.4 copy-start.7
  176.1 5.4 copy-start.2
  176.1 5.4 copy-start.11
  181.5 7.1 %dynamic-slice-start = ((f32[2048]{0:T(1024)}, s32[]{:T(128)}), f32[1024]{0:T(1024)S(1)}, s32[]{:S(2)}) async-start(f32[2048]{0:T(1024)} %param.19, s32[]{:T(128)} %select_n.36), calls=%async_computation.9 | async-start | bytes 8704 | tf_op jit(solution)/shard_map/dynamic_slice | solution.py:67
  181.5 7.1 %dynamic-slice-start.1 = ((f32[2048]{0:T(1024)}, s32[]{:T(128)}), f32[1024]{0:T(1024)S(1)}, s32[]{:S(2)}) async-start(f32[2048]{0:T(1024)} %param.20, s32[]{:T(128)} %select_n.36), calls=%async_computation.10 | async-start | bytes 8704 | tf_op jit(solution)/shard_map/dynamic_slice | solution.py:68
  188.6 1.0 copy-start.10
  215.9 146.7 %all-gather.11.cloned.1.call-start = ((), (), s32[]{:S(2)}) async-start(), calls=%async_computation.4 | async-start | bytes 9437184 | tf_op jit(solution)/shard_map/all_gather | solution.py:105
  216.5 270.8 %all-gather.13.cloned.1.call-start = ((), (), s32[]{:S(2)}) async-start(), calls=%async_computation.5 | async-start | bytes 9437184 | tf_op jit(solution)/shard_map/all_gather | solution.py:106
  217.1 145.6 %copy-start.12 = (f32[2048]{0:T(1024)S(1)}, f32[2048]{0:T(1024)}, u32[]{:S(2)}) copy-start(f32[2048]{0:T(1024)} %param.24) | copy-start | bytes 24580
  217.1 395.3 %all-gather.15.cloned.1.call-start = ((), (), s32[]{:S(2)}) async-start(), calls=%async_computation.6 | async-start | bytes 9437184 | tf_op jit(solution)/shard_map/all_gather | solution.py:112
  217.6 410.6 %reduce-scatter.2.cloned.1.call-start = ((), (), s32[]{:S(2)}) async-start(), calls=%async_computation.7 | async-start | bytes 2359296 | tf_op jit(solution)/shard_map/reduce_scatter | solution.py:113
  237.1 131.5 %copy-start.3 = (bf16[384,2048]{1,0:T(8,128)(2,1)}, bf16[384,2048]{1,0:T(8,128)(2,1)S(1)}, u32[]{:S(2)}) copy-start(bf16[384,2048]{1,0:T(8,128)(2,1)S(1)} %get-tuple-element.10) | copy-start | bytes 4718596
  496.8 131.4 %copy-start.4 = (bf16[384,2048]{1,0:T(8,128)(2,1)S(1)}, bf16[384,2048]{1,0:T(8,128)(2,1)}, u32[]{:S(2)}) copy-start(bf16[384,2048]{1,0:T(8,128)(2,1)} %copy-done.3) | copy-start | bytes 4718596
  620.8 20.9 %all-gather.17.cloned.1.call-start = ((), (), s32[]{:S(2)}) async-start(), calls=%async_computation.8 | async-start | bytes 2359296 | tf_op jit(solution)/shard_map/all_gather | solution.py:120
  620.9 23.6 %copy-start.1 = (f32[16,128]{1,0:T(8,128)S(1)}, f32[16,128]{1,0:T(8,128)}, u32[]{:S(2)}) copy-start(f32[16,128]{1,0:T(8,128)} %param.22) | copy-start | bytes 24580
Sparse Core Ops, SparseCore 0:
  9.5 104.3 all-gather.8
  116.0 90.8 all-gather.6
  216.0 18.9 all-reduce.4
  236.9 125.6 all-gather.10
  364.6 122.6 all-gather.12
  489.2 123.1 all-gather.14
  621.0 7.2 reduce-scatter.1
  630.6 11.0 all-gather.16
